TPU v7x, 32 devices: a whole 2x2x4 slice. The times are simulated.
32 devices in a mesh: ep: 8 (over z, x), tp: 4 (over y, core).
Axes of the slice: x: 2, y: 2, z: 4, core: 2. Of those that a mesh axis runs over, the one named last changes fastest.
Arguments:
- residual: bfloat16 [512, 4096], P('ep', 'tp'), may hold values from -64 to 64
- routes: int32 [512, 2], P('ep'), may hold values from 0 to 7, all different within a row; in each aligned block of 64 rows (0 to 63, 64 to 127, ...) at most 32 rows name the same one
- route_weights: float32 [512, 2], P('ep'), may hold values from 0.2 to 1
- state_prev: float32 [512, 2, 64, 64], P('ep', None, 'tp'), may hold values from -6 to 6
- mix_gain: float32 [4096], replicated, may hold values from 0.1 to 1.9
- ffn_gain: float32 [4096], replicated, may hold values from 0.1 to 1.9
- w_in: bfloat16 [4096, 1024], P(None, 'tp'), may hold values from -0.09375 to 0.09375
- decay_rate: float32 [64, 64], P('tp'), may hold values from 0.5 to 8
- rotation: float32 [64, 64], P('tp'), may hold values from 0 to 200
- log_step: float32 [64], P('tp'), may hold values from -3.9 to -1.2
- in_re: float32 [64, 64, 16], P('tp'), may hold values from -1 to 1
- in_im: float32 [64, 64, 16], P('tp'), may hold values from -1 to 1
- read_re: float32 [64, 16, 64], P('tp'), may hold values from -0.5 to 0.5
- read_im: float32 [64, 16, 64], P('tp'), may hold values from -0.5 to 0.5
- skip_gain: float32 [64, 16], P('tp'), may hold values from -4 to 4
- w_glu: bfloat16 [1024, 1024], P(None, 'tp'), may hold values from -0.1875 to 0.1875
- w_out: bfloat16 [1024, 4096], P('tp'), may hold values from -0.1875 to 0.1875
- w_gate: bfloat16 [8, 4096, 5632], P('ep', None, 'tp'), may hold values from -0.09375 to 0.09375
- w_up: bfloat16 [8, 4096, 5632], P('ep', None, 'tp'), may hold values from -0.09375 to 0.09375
- w_down: bfloat16 [8, 5632, 4096], P('ep', 'tp'), may hold values from -0.078125 to 0.078125
Outputs:
- layer_out: bfloat16 [512, 4096], P('ep', 'tp')
- state_next: float32 [512, 2, 64, 64], P('ep', None, 'tp')
Inputs may be any that keep to these rules, and one draw needn't show every extreme that they name: `routes`: each row names 2 different experts. In each aligned block of 64 rows (the rows of one index of ep) no expert is named more than 32 times, a bound that some block reaches.
All inputs are finite; a program needn't handle non-finite values.
Results may differ from a plain program's by a relative error of at most 0.012.
Values may be sent and summed in bfloat16 or wider, within the bound.
No kernel may reach another device: no remote copies, remote signals or barrier semaphores. Data moves between devices by JAX's collectives and lax.ppermute only.
A program may use at most 128 MiB of HBM per device.

v0:
```python
import jax
import jax.numpy as jnp
from jax import lax
from jax.sharding import PartitionSpec as P

GROUP_CH = 16
TOPK = 2
epsilon = 1e-06
highest = lax.Precision.HIGHEST


def state_mixer(
    u_in, state_prev, decay_rate, rotation, log_step, in_re, in_im, read_re, read_im, skip_gain
):
    batch_rows = u_in.shape[0]
    groups = decay_rate.shape[0]
    grouped = u_in.astype(jnp.float32).reshape(batch_rows, groups, GROUP_CH)
    step_size = jnp.exp(log_step)[:, None]
    real_part = -decay_rate
    magnitude = jnp.exp(real_part * step_size)
    decay_re = magnitude * jnp.cos(rotation * step_size)
    decay_im = magnitude * jnp.sin(rotation * step_size)
    denominator = real_part * real_part + rotation * rotation
    lift_re = ((decay_re - 1.0) * real_part + decay_im * rotation) / denominator
    lift_im = (decay_im * real_part - (decay_re - 1.0) * rotation) / denominator
    map_re = lift_re[..., None] * in_re - lift_im[..., None] * in_im
    map_im = lift_re[..., None] * in_im + lift_im[..., None] * in_re
    drive_re = jnp.einsum("gph,bgh->bgp", map_re, grouped, precision=highest)
    drive_im = jnp.einsum("gph,bgh->bgp", map_im, grouped, precision=highest)
    old_re = state_prev[:, 0]
    old_im = state_prev[:, 1]
    new_re = decay_re * old_re - decay_im * old_im + drive_re
    new_im = decay_re * old_im + decay_im * old_re + drive_im
    output = (
        jnp.einsum("ghp,bgp->bgh", read_re, new_re, precision=highest)
        - jnp.einsum("ghp,bgp->bgh", read_im, new_im, precision=highest)
        + skip_gain * grouped
    )
    return (jax.nn.gelu(output.reshape(batch_rows, -1)), jnp.stack([new_re, new_im], axis=1))


def per_device(
    residual,
    routes,
    route_weights,
    state_prev,
    mix_gain,
    ffn_gain,
    w_in,
    decay_rate,
    rotation,
    log_step,
    in_re,
    in_im,
    read_re,
    read_im,
    skip_gain,
    w_glu,
    w_out,
    w_gate,
    w_up,
    w_down,
):
    shard_width = residual.shape[1]
    full_width = shard_width * lax.axis_size("tp")
    tp_place = lax.axis_index("tp")
    experts_all = lax.axis_size("ep")
    seq_rows = residual.shape[0]
    capacity = 2 * seq_rows * TOPK // experts_all
    source = residual.astype(jnp.float32)
    squares = lax.psum(jnp.sum(source * source, axis=1), "tp")
    own_gain = lax.dynamic_slice_in_dim(mix_gain, tp_place * shard_width, shard_width)
    scale_rows = lax.rsqrt(squares / full_width + epsilon)[:, None]
    outgoing = (source * scale_rows * own_gain).astype(jnp.bfloat16)
    gathered = lax.all_gather(outgoing, "tp", axis=1, tiled=True)
    u_in = jnp.dot(gathered, w_in, preferred_element_type=jnp.float32).astype(jnp.bfloat16)
    mixer_act, state_next = state_mixer(
        u_in, state_prev, decay_rate, rotation, log_step, in_re, in_im, read_re, read_im, skip_gain
    )
    mixer_bf = mixer_act.astype(jnp.bfloat16)
    all_channels = lax.all_gather(mixer_bf, "tp", axis=1, tiled=True)
    glu_logit = jnp.dot(all_channels, w_glu, preferred_element_type=jnp.float32)
    mixed = (mixer_act * jax.nn.sigmoid(glu_logit)).astype(jnp.bfloat16)
    partial_out = jnp.dot(mixed, w_out, preferred_element_type=jnp.float32)
    branch = lax.psum_scatter(
        partial_out.astype(jnp.bfloat16), "tp", scatter_dimension=1, tiled=True
    ).astype(jnp.float32)
    after_float = (source + branch).astype(jnp.bfloat16).astype(jnp.float32)
    squares_ffn = lax.psum(jnp.sum(after_float * after_float, axis=1), "tp")
    ffn_own = lax.dynamic_slice_in_dim(ffn_gain, tp_place * shard_width, shard_width)
    scale_ffn = lax.rsqrt(squares_ffn / full_width + epsilon)[:, None]
    normed_ffn = (after_float * scale_ffn * ffn_own).astype(jnp.bfloat16)
    flat_routes = routes.reshape(-1)
    onehot = (flat_routes[:, None] == jnp.arange(experts_all, dtype=jnp.int32)).astype(jnp.int32)
    before = jnp.cumsum(onehot, axis=0) - onehot
    slot_index = jnp.sum(before * onehot, axis=1)
    destination = (flat_routes * capacity + slot_index).reshape(seq_rows, TOPK)
    matches = destination[:, :, None] == jnp.arange(experts_all * capacity, dtype=jnp.int32)
    dispatch_map = jnp.sum(matches.astype(jnp.float32), axis=1).astype(jnp.bfloat16)
    combine_map = jnp.sum(jnp.where(matches, route_weights[:, :, None], 0.0), axis=1)
    outbound = jnp.einsum("bj,bd->jd", dispatch_map, normed_ffn, preferred_element_type=jnp.float32)
    outbound = outbound.astype(jnp.bfloat16).reshape(experts_all, capacity, shard_width)
    arrived = lax.all_gather(
        lax.all_to_all(outbound, "ep", split_axis=0, concat_axis=0, tiled=True),
        "tp",
        axis=2,
        tiled=True,
    )
    sources, slots_here, row_width = arrived.shape
    flat_rows = arrived.reshape(sources * slots_here, row_width)
    gate_value = jnp.dot(flat_rows, w_gate[0], preferred_element_type=jnp.float32)
    up_value = jnp.dot(flat_rows, w_up[0], preferred_element_type=jnp.float32)
    hidden = (jax.nn.silu(gate_value) * up_value).astype(jnp.bfloat16)
    partial_sum = jnp.dot(hidden, w_down[0], preferred_element_type=jnp.float32)
    partial_sum = partial_sum.reshape(sources, slots_here, row_width)
    reduced = lax.psum_scatter(
        partial_sum.astype(jnp.bfloat16), "tp", scatter_dimension=2, tiled=True
    )
    came_back = lax.all_to_all(reduced, "ep", split_axis=0, concat_axis=0, tiled=True)
    came_back = came_back.reshape(experts_all * capacity, shard_width).astype(jnp.float32)
    combined = jnp.dot(combine_map, came_back, precision=highest)
    layer_out = (after_float + combined).astype(jnp.bfloat16)
    return (layer_out, state_next)


def solution(mesh):
    return jax.shard_map(
        per_device,
        mesh=mesh,
        in_specs=(
            P("ep", "tp"),
            P("ep", None),
            P("ep", None),
            P("ep", None, "tp", None),
            P(),
            P(),
            P(None, "tp"),
            P("tp", None),
            P("tp", None),
            P("tp"),
            P("tp", None, None),
            P("tp", None, None),
            P("tp", None, None),
            P("tp", None, None),
            P("tp", None),
            P(None, "tp"),
            P("tp", None),
            P("ep", None, "tp"),
            P("ep", None, "tp"),
            P("ep", "tp", None),
        ),
        out_specs=(P("ep", "tp"), P("ep", None, "tp", None)),
        check_vma=False,
    )
```

profile of v0, /device:TPU:0, one launch (start us, length us, event | category | flops | bytes accessed | tf_op | source)
XLA Modules:
  0.0 192.4 jit_solution(10713720667919204251)
XLA Ops:
  7.2 0.0 copy-start
  7.2 0.0 reduce-scatter.3.cloned.1.call-start
  7.2 0.8 exp.13
  8.0 1.0 fusion.25
  9.1 8.4 %psum.14 = f32[64]{0:T(128)S(1)} all-reduce(f32[64]{0:T(128)S(1)} %fusion.25), channel_id=1, replica_groups=mesh['ep'=8,'tp'=4] {'tp'}, use_global_device_ids=true, to_apply=%region_1.0 | all-reduce | flops 64 | bytes 512 | tf_op jit(solution)/shard_map/psum | solution.py:71
  17.5 0.7 dynamic_slice.6
  18.2 1.0 fusion.27
  19.2 6.5 %all_gather.9 = bf16[64,4096]{1,0:T(8,128)(2,1)S(1)} all-gather(bf16[64,1024]{1,0:T(8,128)(2,1)S(1)} %fusion.27), channel_id=1, replica_groups=mesh['ep'=8,'tp'=4] {'tp'}, dimensions={1}, use_global_device_ids=true | all-gather | bytes 655360 | tf_op jit(solution)/shard_map/all_gather | solution.py:75
  25.7 2.1 %convolution_convert_fusion.2 = bf16[64,256]{1,0:T(8,128)(2,1)S(1)} fusion(bf16[64,4096]{1,0:T(8,128)(2,1)S(1)} %all_gather.9, bf16[4096,256]{1,0:T(8,128)(2,1)} %param.26), kind=kOutput, calls=%fused_computation.26 | convolution fusion | flops 134234112 | bytes 2654208 | tf_op jit(solution)/shard_map/dot_general | solution.py:76
  27.8 0.1 copy.55
  27.9 1.3 fusion.62
  29.2 0.0 copy-done.8
  29.2 0.0 copy-done.9
  29.2 0.0 copy-start.6
  29.2 0.1 add_divide_fusion
  29.3 0.0 copy-done.3
  29.4 0.0 copy-done.4
  29.4 0.0 copy-start.5
  29.4 0.0 copy-start.7
  29.4 0.7 fusion.15
  30.1 0.7 fusion.16
  30.7 0.0 copy-done.6
  30.7 0.9 fusion.63
  31.7 0.0 copy-done.5
  31.7 0.0 copy-done.7
  31.7 0.9 fusion.19
  32.6 0.1 copy.60
  32.7 0.0 copy-start.10
  32.7 5.4 %all_gather.10 = bf16[64,1024]{1,0:T(8,128)(2,1)S(1)} all-gather(bf16[64,256]{1,0:T(8,128)(2,1)S(1)} %fusion.56), channel_id=1, replica_groups=mesh['ep'=8,'tp'=4] {'tp'}, dimensions={1}, use_global_device_ids=true | all-gather | bytes 163840 | tf_op jit(solution)/shard_map/all_gather | solution.py:81
  38.2 0.0 copy-done
  38.2 2.7 %convolution_convert_fusion = bf16[64,4096]{1,0:T(8,128)(2,1)} fusion(bf16[256,4096]{1,0:T(8,128)(2,1)S(1)} %copy-done, bf16[64,1024]{1,0:T(8,128)(2,1)S(1)} %all_gather.10, bf16[1024,256]{1,0:T(8,128)(2,1)} %param.35, f32[64,256]{1,0:T(8,128)S(1)} %copy.60), kind=kOutput, calls=%fused_computation.7 | convolution fusion | flops 168247296 | bytes 3342336 | tf_op jit(solution)/shard_map/dot_general | solution.py:84
  40.8 0.0 reduce-scatter.3.cloned.1.call-update
  40.9 0.0 all-gather.2.cloned.1.call-start
  40.9 0.0 copy-done.10
  40.9 0.1 copy.61
  41.0 0.1 eq.28
  41.2 0.1 fusion.48
  41.3 0.2 reduce_window_sum.11
  41.4 0.2 select_reduce_fusion.1
  41.6 0.1 reduce_sum.49
  41.8 0.1 copy.62
  41.8 0.0 copy-done.11
  41.8 0.1 convert_reduce_fusion
  42.0 21.7 %reduce-scatter.3.cloned.1.call-done = bf16[64,1024]{1,0:T(8,128)(2,1)} async-done(((bf16[64,4096]{1,0:T(8,128)(2,1)}), bf16[64,1024]{1,0:T(8,128)(2,1)}) %reduce-scatter.3.cloned.1.call-update) | async-done | bytes 131088 | tf_op jit(solution)/shard_map/reduce_scatter | solution.py:85
  63.6 0.0 copy-done.1
  63.6 1.0 fusion.29
  64.7 5.8 %psum.15 = f32[64]{0:T(128)S(1)} all-reduce(f32[64]{0:T(128)S(1)} %fusion.29), channel_id=1, replica_groups=mesh['ep'=8,'tp'=4] {'tp'}, use_global_device_ids=true, to_apply=%region_8.9 | all-reduce | flops 64 | bytes 512 | tf_op jit(solution)/shard_map/psum | solution.py:89
  70.5 0.0 dynamic-slice-done
  70.5 1.2 convolution_convert_fusion.1
  71.7 19.8 %all_to_all.10 = bf16[8,32,1024]{2,1,0:T(8,128)(2,1)} all-to-all(bf16[8,32,1024]{2,1,0:T(8,128)(2,1)S(1)} %bitcast.67), channel_id=1, replica_groups=mesh['ep'=8,'tp'=4] {'ep'}, dimensions={0} | all-to-all | bytes 1048576 | tf_op jit(solution)/shard_map/all_to_all | solution.py:104
  91.6 0.0 all-gather.2.cloned.1.call-update
  91.6 0.0 reduce-scatter.5.cloned.1.call-start
  91.6 20.8 %all-gather.2.cloned.1.call-done = bf16[8,32,4096]{2,1,0:T(8,128)(2,1)} async-done(((bf16[8,32,1024]{2,1,0:T(8,128)(2,1)}), bf16[8,32,4096]{2,1,0:T(8,128)(2,1)}) %all-gather.2.cloned.1.call-update) | async-done | bytes 2097168 | tf_op jit(solution)/shard_map/all_gather | solution.py:103
  112.4 7.4 %fusion.4 = f32[256,1408]{1,0:T(8,128)S(1)} fusion(bf16[256,4096]{1,0:T(8,128)(2,1)} %bitcast.74, bf16[1,4096,1408]{2,1,0:T(8,128)(2,1)} %param.37), kind=kOutput, calls=%fused_computation.4 | convolution fusion | flops 2952790016 | bytes 15073280 | tf_op jit(solution)/shard_map/dot_general | solution.py:111
  119.9 0.0 slice-start.2
  119.9 8.0 %fusion.12 = bf16[256,1408]{1,0:T(8,128)(2,1)S(1)} fusion(bf16[256,4096]{1,0:T(8,128)(2,1)S(1)} %bitcast.75, bf16[1,4096,1408]{2,1,0:T(8,128)(2,1)} %param.38, f32[256,1408]{1,0:T(8,128)S(1)} %fusion.4), kind=kOutput, calls=%fused_computation.9 | convolution fusion | flops 2954952704 | bytes 15794176 | tf_op jit(solution)/shard_map/dot_general | solution.py:112
  127.9 4.6 %fusion.6 = bf16[8,32,4096]{2,1,0:T(8,128)(2,1)} fusion(bf16[8,32,1408]{2,1,0:T(8,128)(2,1)S(1)} %bitcast.76, bf16[1,1408,4096]{2,1,0:T(8,128)(2,1)S(1)} %bitcast.73), kind=kOutput, calls=%fused_computation.6 | convolution fusion | flops 2953838592 | bytes 14352384 | tf_op jit(solution)/shard_map/dot_general | solution.py:114
  132.5 0.0 reduce-scatter.5.cloned.1.call-update
  132.6 31.3 %reduce-scatter.5.cloned.1.call-done = bf16[8,32,1024]{2,1,0:T(8,128)(2,1)} async-done(((bf16[8,32,4096]{2,1,0:T(8,128)(2,1)}), bf16[8,32,1024]{2,1,0:T(8,128)(2,1)}) %reduce-scatter.5.cloned.1.call-update) | async-done | bytes 524304 | tf_op jit(solution)/shard_map/reduce_scatter | solution.py:116
  163.9 5.5 %all-to-all-start.1 = ((bf16[8,32,1024]{2,1,0:T(8,128)(2,1)}), bf16[8,32,1024]{2,1,0:T(8,128)(2,1)}, u32[]{:S(2)}, u32[]{:S(2)}) async-start(bf16[8,32,1024]{2,1,0:T(8,128)(2,1)} %reduce-scatter.5.cloned.1.call-done), calls=%async_computation.3 | async-start | bytes 1048576 | tf_op jit(solution)/shard_map/all_to_all | solution.py:119
  169.4 0.1 pad_maximum_fusion
  169.5 1.6 copy.63
  171.1 12.7 %all-to-all-done.1 = bf16[8,32,1024]{2,1,0:T(8,128)(2,1)} async-done(((bf16[8,32,1024]{2,1,0:T(8,128)(2,1)}), bf16[8,32,1024]{2,1,0:T(8,128)(2,1)}, u32[]{:S(2)}, u32[]{:S(2)}) %all-to-all-start.1) | async-done | bytes 524320 | tf_op jit(solution)/shard_map/all_to_all | solution.py:119
  183.8 2.1 %fusion.17 = bf16[64,1024]{1,0:T(8,128)(2,1)} fusion(f32[64,256]{1,0:T(8,128)S(1)} %get-tuple-element.11, bf16[256,1024]{1,0:T(8,128)(2,1)} %bitcast.14, bf16[64,1024]{1,0:T(8,128)(2,1)S(1)} %copy-done.2, bf16[64,1024]{1,0:T(8,128)(2,1)S(1)} %copy-done.1), kind=kOutput, calls=%fused_computation.16 | convolution fusion | flops 201785344 | bytes 983040 | tf_op jit(solution)/shard_map/dot_general | solution.py:121
  (21 shorter events, 0.1 us)
Async XLA Ops:
  7.2 31.0 %copy-start = (bf16[256,4096]{1,0:T(8,128)(2,1)S(1)}, bf16[256,4096]{1,0:T(8,128)(2,1)}, u32[]{:S(2)}) copy-start(bf16[256,4096]{1,0:T(8,128)(2,1)} %param.36) | copy-start | bytes 6291460
  7.2 56.5 %reduce-scatter.3.cloned.1.call-start = ((), (), s32[]{:S(2)}) async-start(), calls=%async_computation.4 | async-start | bytes 655360 | tf_op jit(solution)/shard_map/reduce_scatter | solution.py:85
  25.7 3.5 %copy-start.8 = (f32[16,64]{1,0:T(8,128)S(1)}, f32[16,64]{1,0:T(8,128)}, u32[]{:S(2)}) copy-start(f32[16,64]{1,0:T(8,128)} %param.28) | copy-start | bytes 12292
  25.7 3.5 %copy-start.9 = (f32[16,64]{1,0:T(8,128)S(1)}, f32[16,64]{1,0:T(8,128)}, u32[]{:S(2)}) copy-start(f32[16,64]{1,0:T(8,128)} %param.27) | copy-start | bytes 12292
  25.7 3.7 %copy-start.3 = (f32[16,64,16]{1,2,0:T(8,128)S(1)}, f32[16,64,16]{1,2,0:T(8,128)}, u32[]{:S(2)}) copy-start(f32[16,64,16]{1,2,0:T(8,128)} %param.31) | copy-start | bytes 196612
  25.7 3.7 %copy-start.4 = (f32[16,64,16]{1,2,0:T(8,128)S(1)}, f32[16,64,16]{1,2,0:T(8,128)}, u32[]{:S(2)}) copy-start(f32[16,64,16]{1,2,0:T(8,128)} %param.30) | copy-start | bytes 196612
  29.2 1.5 copy-start.6
  29.4 2.3 %copy-start.5 = (f32[16,16,64]{2,1,0:T(8,128)S(1)}, f32[16,16,64]{2,1,0:T(8,128)}, u32[]{:S(2)}) copy-start(f32[16,16,64]{2,1,0:T(8,128)} %param.33) | copy-start | bytes 196612
  29.4 2.3 %copy-start.7 = (f32[16,16]{1,0:T(8,128)S(1)}, f32[16,16]{1,0:T(8,128)}, u32[]{:S(2)}) copy-start(f32[16,16]{1,0:T(8,128)} %param.34) | copy-start | bytes 3076
  32.7 8.2 %copy-start.10 = (s32[64,2]{0,1:T(2,128)S(1)}, s32[64,2]{0,1:T(2,128)}, u32[]{:S(2)}) copy-start(s32[64,2]{0,1:T(2,128)} %param.21) | copy-start | bytes 1540
  38.2 3.7 %copy-start.11 = (f32[64,2]{0,1:T(2,128)S(1)}, f32[64,2]{0,1:T(2,128)}, u32[]{:S(2)}) copy-start(f32[64,2]{0,1:T(2,128)} %param.22) | copy-start | bytes 1540
  38.2 25.5 %copy-start.1 = (bf16[64,1024]{1,0:T(8,128)(2,1)S(1)}, bf16[64,1024]{1,0:T(8,128)(2,1)}, u32[]{:S(2)}) copy-start(bf16[64,1024]{1,0:T(8,128)(2,1)} %param.20) | copy-start | bytes 393220
  38.2 32.3 %dynamic-slice-start = ((f32[4096]{0:T(1024)}, s32[]{:T(128)}), f32[1024]{0:T(1024)S(1)}, s32[]{:S(2)}) async-start(f32[4096]{0:T(1024)} %param.25, s32[]{:T(128)} %select_n.8), calls=%async_computation.7 | async-start | bytes 8704 | tf_op jit(solution)/shard_map/dynamic_slice | solution.py:90
  40.9 71.6 %all-gather.2.cloned.1.call-start = ((), (), s32[]{:S(2)}) async-start(), calls=%async_computation.5 | async-start | bytes 2621440 | tf_op jit(solution)/shard_map/all_gather | solution.py:103
  91.6 72.3 %reduce-scatter.5.cloned.1.call-start = ((), (), s32[]{:S(2)}) async-start(), calls=%async_computation.6 | async-start | bytes 2621440 | tf_op jit(solution)/shard_map/reduce_scatter | solution.py:116
  112.4 7.4 %copy-start.12 = (bf16[8,32,4096]{2,1,0:T(8,128)(2,1)S(1)}, bf16[8,32,4096]{2,1,0:T(8,128)(2,1)}, u32[]{:S(2)}) copy-start(bf16[8,32,4096]{2,1,0:T(8,128)(2,1)} %all-gather.2.cloned.1.call-done) | copy-start | bytes 6291460
  112.4 15.5 %slice-start = ((s8[11534336]{0:T(1024)(128)(4,1)}), s8[4194304]{0:T(1024)(128)(4,1)S(1)}, s32[]{:S(2)}) async-start(s8[11534336]{0:T(1024)(128)(4,1)} %bitcast.72), calls=%async_computation.8 | async-start | bytes 8388608
  112.4 15.5 %slice-start.1 = ((s8[11534336]{0:T(1024)(128)(4,1)}), s8[4194304]{0:T(1024)(128)(4,1)S(1)}, s32[]{:S(2)}) async-start(s8[11534336]{0:T(1024)(128)(4,1)} %bitcast.72), calls=%async_computation.9 | async-start | bytes 8388608
  119.9 8.0 %slice-start.2 = ((s8[11534336]{0:T(1024)(128)(4,1)}), s8[3145728]{0:T(1024)(128)(4,1)S(1)}, s32[]{:S(2)}) async-start(s8[11534336]{0:T(1024)(128)(4,1)} %bitcast.72), calls=%async_computation.10 | async-start | bytes 6291456
  163.9 19.9 %all-to-all-start.1 = ((bf16[8,32,1024]{2,1,0:T(8,128)(2,1)}), bf16[8,32,1024]{2,1,0:T(8,128)(2,1)}, u32[]{:S(2)}, u32[]{:S(2)}) async-start(bf16[8,32,1024]{2,1,0:T(8,128)(2,1)} %reduce-scatter.5.cloned.1.call-done), calls=%async_computation.3 | async-start | bytes 1048576 | tf_op jit(solution)/shard_map/all_to_all | solution.py:119
  169.4 14.4 %copy-start.2 = (bf16[64,1024]{1,0:T(8,128)(2,1)S(1)}, bf16[64,1024]{1,0:T(8,128)(2,1)}, u32[]{:S(2)}) copy-start(bf16[64,1024]{1,0:T(8,128)(2,1)} %reduce-scatter.3.cloned.1.call-done) | copy-start | bytes 393220
Sparse Core Ops, SparseCore 0:
  41.0 22.5 reduce-scatter.2
  91.7 20.6 all-gather.1
  132.7 31.1 reduce-scatter.4
where the time goes:
time: 193 us; the launch traced here: 192 us
  waiting for transfers between devices  86.5 us (45%)
  blocking collectives  45.9 us (24%)
  matrix products  31.3 us (16%)
  between operations  14 us (7%)
  starting transfers between devices  5.63 us (3%)
  local copies, waits for them, and re-layouts  5.09 us (3%)
  other arithmetic  3.92 us (2%)
    reduce_scatter x1, waiting for transfers between devices, per_device(): lax.psum_scatter(partial_sum.astype(jnp.bfloat16), 'tp', scatter_dimensio...  31.3 us
    reduce_scatter x1, waiting for transfers between devices, per_device(): lax.psum_scatter(partial_out.astype(jnp.bfloat16), 'tp', scatter_dimensio...  21.7 us
    all_gather x1, waiting for transfers between devices, per_device(): lax.all_gather(lax.all_to_all(outbound, 'ep', split_axis=0, concat_axis=0...  20.8 us
    all_to_all x1, blocking collectives, per_device(): lax.all_to_all(outbound, 'ep', split_axis=0, concat_axis=0, tiled=True)  19.8 us
    all_to_all x1, waiting for transfers between devices, per_device(): lax.all_to_all(reduced, 'ep', split_axis=0, concat_axis=0, tiled=True)  12.7 us
    psum x1, blocking collectives, per_device(): squares = lax.psum(jnp.sum(source * source, axis=1), 'tp')  8.4 us
    dot_general x1, matrix products, per_device(): up_value = jnp.dot(flat_rows, w_up[0], preferred_element_type=jnp.float32)  8.01 us
    dot_general x1, matrix products, per_device(): jnp.dot(flat_rows, w_gate[0], preferred_element_type=jnp.float32)  7.42 us
  transfers between devices with their start and end apart: 4, of which 4 were waited for; matrix products, arithmetic and copies ran while one was open for 1% of the time, Pallas kernels for 0%

commit v1 on v0

--- a/solution.py
+++ b/solution.py
@@ -100,11 +100,11 @@
     combine_map = jnp.sum(jnp.where(matches, route_weights[:, :, None], 0.0), axis=1)
     outbound = jnp.einsum("bj,bd->jd", dispatch_map, normed_ffn, preferred_element_type=jnp.float32)
     outbound = outbound.astype(jnp.bfloat16).reshape(experts_all, capacity, shard_width)
-    arrived = lax.all_gather(
-        lax.all_to_all(outbound, "ep", split_axis=0, concat_axis=0, tiled=True),
-        "tp",
+    arrived = jnp.concatenate(
+        lax.all_gather(
+            lax.all_to_all(outbound, "ep", split_axis=0, concat_axis=0, tiled=True), "tp"
+        ),
         axis=2,
-        tiled=True,
     )
     sources, slots_here, row_width = arrived.shape
     flat_rows = arrived.reshape(sources * slots_here, row_width)

time: 193 us -> 192 us (level)
  matrix products: 31.3 us -> 26.2 us
  local copies, waits for them, and re-layouts: 5.09 us -> 9.41 us
    dot_general x1, matrix products: 8.01 us -> 3.5 us  [per_device(): up_value = jnp.dot(flat_rows, w_up[0], preferred_element_type=jnp.float32)]
    reshape x0 -> x1, local copies, waits for them, and re-layouts: none -> 3.22 us  [per_device(): jnp.concatenate(lax.all_gather(lax.all_to_all(outbound, 'ep', split_axis=...]
where the time goes in v1:
time: 192 us
  waiting for transfers between devices  86.4 us (45%)
  blocking collectives  45.9 us (24%)
  matrix products  26.2 us (14%)
  between operations  14.1 us (7%)
  local copies, waits for them, and re-layouts  9.41 us (5%)
  starting transfers between devices  5.81 us (3%)
  other arithmetic  3.92 us (2%)
    reduce_scatter x1, waiting for transfers between devices, per_device(): lax.psum_scatter(partial_sum.astype(jnp.bfloat16), 'tp', scatter_dimensio...  31.3 us
    reduce_scatter x1, waiting for transfers between devices, per_device(): lax.psum_scatter(partial_out.astype(jnp.bfloat16), 'tp', scatter_dimensio...  21.7 us
    all_gather x1, waiting for transfers between devices, per_device(): lax.all_gather(lax.all_to_all(outbound, 'ep', split_axis=0, concat_axis=0...  20.6 us
    all_to_all x1, blocking collectives, per_device(): lax.all_to_all(outbound, 'ep', split_axis=0, concat_axis=0, tiled=True)  19.8 us
    all_to_all x1, waiting for transfers between devices, per_device(): lax.all_to_all(reduced, 'ep', split_axis=0, concat_axis=0, tiled=True)  12.7 us
    psum x1, blocking collectives, per_device(): squares = lax.psum(jnp.sum(source * source, axis=1), 'tp')  8.4 us
    dot_general x1, matrix products, per_device(): jnp.dot(flat_rows, w_gate[0], preferred_element_type=jnp.float32)  6.73 us
    all_gather x1, blocking collectives, per_device(): gathered = lax.all_gather(outgoing, 'tp', axis=1, tiled=True)  6.5 us
  transfers between devices with their start and end apart: 4, of which 4 were waited for; matrix products, arithmetic and copies ran while one was open for 1% of the time, Pallas kernels for 0%

profile of v1, /device:TPU:0, one launch (start us, length us, event | category | flops | bytes accessed | tf_op | source)
XLA Modules:
  0.0 191.7 jit_solution(4413990284348459242)
XLA Ops:
  7.2 0.0 copy-start
  7.2 0.0 reduce-scatter.3.cloned.1.call-start
  7.2 0.8 exp.13
  8.0 1.0 fusion.25
  9.1 8.4 %psum.14 = f32[64]{0:T(128)S(1)} all-reduce(f32[64]{0:T(128)S(1)} %fusion.25), channel_id=1, replica_groups=mesh['ep'=8,'tp'=4] {'tp'}, use_global_device_ids=true, to_apply=%region_1.0 | all-reduce | flops 64 | bytes 512 | tf_op jit(solution)/shard_map/psum | solution.py:71
  17.5 0.7 dynamic_slice.6
  18.2 1.0 fusion.27
  19.2 6.5 %all_gather.12 = bf16[64,4096]{1,0:T(8,128)(2,1)S(1)} all-gather(bf16[64,1024]{1,0:T(8,128)(2,1)S(1)} %fusion.27), channel_id=1, replica_groups=mesh['ep'=8,'tp'=4] {'tp'}, dimensions={1}, use_global_device_ids=true | all-gather | bytes 655360 | tf_op jit(solution)/shard_map/all_gather | solution.py:75
  25.7 2.1 %convolution_convert_fusion.2 = bf16[64,256]{1,0:T(8,128)(2,1)S(1)} fusion(bf16[64,4096]{1,0:T(8,128)(2,1)S(1)} %all_gather.12, bf16[4096,256]{1,0:T(8,128)(2,1)} %param.26), kind=kOutput, calls=%fused_computation.26 | convolution fusion | flops 134234112 | bytes 2654208 | tf_op jit(solution)/shard_map/dot_general | solution.py:76
  27.8 0.1 copy.84
  27.9 1.3 fusion.62
  29.2 0.0 copy-done.8
  29.2 0.0 copy-done.9
  29.2 0.0 copy-start.6
  29.2 0.1 add_divide_fusion
  29.4 0.0 copy-done.3
  29.4 0.0 copy-start.5
  29.4 0.0 copy-start.7
  29.4 0.7 fusion.15
  30.1 0.7 fusion.16
  30.7 0.9 fusion.63
  31.7 0.9 fusion.19
  32.6 0.1 copy.89
  32.7 0.0 copy-start.10
  32.8 5.4 %all_gather.13 = bf16[64,1024]{1,0:T(8,128)(2,1)S(1)} all-gather(bf16[64,256]{1,0:T(8,128)(2,1)S(1)} %fusion.56), channel_id=1, replica_groups=mesh['ep'=8,'tp'=4] {'tp'}, dimensions={1}, use_global_device_ids=true | all-gather | bytes 163840 | tf_op jit(solution)/shard_map/all_gather | solution.py:81
  38.2 2.7 %convolution_convert_fusion = bf16[64,4096]{1,0:T(8,128)(2,1)} fusion(bf16[256,4096]{1,0:T(8,128)(2,1)S(1)} %copy-done, bf16[64,1024]{1,0:T(8,128)(2,1)S(1)} %all_gather.13, bf16[1024,256]{1,0:T(8,128)(2,1)} %param.35, f32[64,256]{1,0:T(8,128)S(1)} %copy.89), kind=kOutput, calls=%fused_computation.7 | convolution fusion | flops 168247296 | bytes 3342336 | tf_op jit(solution)/shard_map/dot_general | solution.py:84
  40.9 0.0 reduce-scatter.3.cloned.1.call-update
  40.9 0.0 all-gather.3.cloned.1.call-start
  40.9 0.1 copy.90
  41.0 0.1 eq.28
  41.2 0.1 fusion.48
  41.3 0.2 reduce_window_sum.11
  41.4 0.2 select_reduce_fusion.1
  41.6 0.1 reduce_sum.49
  41.8 0.1 copy.91
  41.8 0.0 copy-done.11
  41.8 0.1 convert_reduce_fusion
  42.0 21.7 %reduce-scatter.3.cloned.1.call-done = bf16[64,1024]{1,0:T(8,128)(2,1)} async-done(((bf16[64,4096]{1,0:T(8,128)(2,1)}), bf16[64,1024]{1,0:T(8,128)(2,1)}) %reduce-scatter.3.cloned.1.call-update) | async-done | bytes 131088 | tf_op jit(solution)/shard_map/reduce_scatter | solution.py:85
  63.6 1.0 fusion.29
  64.7 5.8 %psum.15 = f32[64]{0:T(128)S(1)} all-reduce(f32[64]{0:T(128)S(1)} %fusion.29), channel_id=1, replica_groups=mesh['ep'=8,'tp'=4] {'tp'}, use_global_device_ids=true, to_apply=%region_8.9 | all-reduce | flops 64 | bytes 512 | tf_op jit(solution)/shard_map/psum | solution.py:89
  70.5 0.0 dynamic-slice-done
  70.5 1.3 convolution_convert_fusion.1
  71.7 19.8 %all_to_all.10 = bf16[8,32,1024]{2,1,0:T(8,128)(2,1)} all-to-all(bf16[8,32,1024]{2,1,0:T(8,128)(2,1)S(1)} %bitcast.76), channel_id=1, replica_groups=mesh['ep'=8,'tp'=4] {'ep'}, dimensions={0} | all-to-all | bytes 1048576 | tf_op jit(solution)/shard_map/all_to_all | solution.py:105
  91.5 0.0 all-gather.3.cloned.1.call-update
  91.6 0.2 reduce-scatter.5.cloned.1.call-start
  91.8 20.6 %all-gather.3.cloned.1.call-done = bf16[32,32,1024]{2,1,0:T(8,128)(2,1)} async-done(((bf16[8,32,1024]{2,1,0:T(8,128)(2,1)}), bf16[32,32,1024]{2,1,0:T(8,128)(2,1)}) %all-gather.3.cloned.1.call-update) | async-done | bytes 2097168 | tf_op jit(solution)/shard_map/all_gather | solution.py:104
  112.4 3.2 %copy.92 = bf16[8,32,4,1024]{3,2,1,0:T(4,128)(2,1)S(1)} copy(bf16[8,32,4,1024]{3,1,0,2:T(8,128)(2,1)} %bitcast.73) | data formatting | bytes 4194304 | tf_op jit(solution)/shard_map/reshape | solution.py:103
  115.6 0.0 slice-start
  115.7 0.9 copy.96
  116.5 0.0 slice-start.1
  116.5 0.0 slice-start.2
  116.6 0.0 slice-start.3
  116.6 0.0 slice-start.4
  116.6 6.7 %fusion.4 = f32[256,1408]{1,0:T(8,128)S(1)} fusion(bf16[256,4096]{1,0:T(8,128)(2,1)S(1)} %bitcast.74, bf16[1,4096,1408]{2,1,0:T(8,128)(2,1)} %param.37), kind=kOutput, calls=%fused_computation.4 | convolution fusion | flops 2952790016 | bytes 15073280 | tf_op jit(solution)/shard_map/dot_general | solution.py:111
  123.3 0.2 slice-done.2
  123.6 3.5 %fusion.12 = bf16[256,1408]{1,0:T(8,128)(2,1)S(1)} fusion(bf16[256,4096]{1,0:T(8,128)(2,1)S(1)} %bitcast.75, bf16[1,4096,1408]{2,1,0:T(8,128)(2,1)S(1)} %bitcast.82, f32[256,1408]{1,0:T(8,128)S(1)} %fusion.4), kind=kOutput, calls=%fused_computation.9 | convolution fusion | flops 2954952704 | bytes 15794176 | tf_op jit(solution)/shard_map/dot_general | solution.py:112
  127.1 4.7 %fusion.6 = bf16[8,32,4096]{2,1,0:T(8,128)(2,1)} fusion(bf16[8,32,1408]{2,1,0:T(8,128)(2,1)S(1)} %bitcast.85, bf16[1,1408,4096]{2,1,0:T(8,128)(2,1)S(1)} %bitcast.84), kind=kOutput, calls=%fused_computation.6 | convolution fusion | flops 2953838592 | bytes 14352384 | tf_op jit(solution)/shard_map/dot_general | solution.py:114
  131.8 0.0 reduce-scatter.5.cloned.1.call-update
  131.8 31.3 %reduce-scatter.5.cloned.1.call-done = bf16[8,32,1024]{2,1,0:T(8,128)(2,1)} async-done(((bf16[8,32,4096]{2,1,0:T(8,128)(2,1)}), bf16[8,32,1024]{2,1,0:T(8,128)(2,1)}) %reduce-scatter.5.cloned.1.call-update) | async-done | bytes 524304 | tf_op jit(solution)/shard_map/reduce_scatter | solution.py:116
  163.1 5.5 %all-to-all-start.1 = ((bf16[8,32,1024]{2,1,0:T(8,128)(2,1)}), bf16[8,32,1024]{2,1,0:T(8,128)(2,1)}, u32[]{:S(2)}, u32[]{:S(2)}) async-start(bf16[8,32,1024]{2,1,0:T(8,128)(2,1)} %reduce-scatter.5.cloned.1.call-done), calls=%async_computation.3 | async-start | bytes 1048576 | tf_op jit(solution)/shard_map/all_to_all | solution.py:119
  168.6 0.1 pad_maximum_fusion
  168.8 1.6 copy.93
  170.3 12.7 %all-to-all-done.1 = bf16[8,32,1024]{2,1,0:T(8,128)(2,1)} async-done(((bf16[8,32,1024]{2,1,0:T(8,128)(2,1)}), bf16[8,32,1024]{2,1,0:T(8,128)(2,1)}, u32[]{:S(2)}, u32[]{:S(2)}) %all-to-all-start.1) | async-done | bytes 524320 | tf_op jit(solution)/shard_map/all_to_all | solution.py:119
  183.1 2.1 %fusion.17 = bf16[64,1024]{1,0:T(8,128)(2,1)} fusion(f32[64,256]{1,0:T(8,128)S(1)} %get-tuple-element.15, bf16[256,1024]{1,0:T(8,128)(2,1)} %bitcast.15, bf16[64,1024]{1,0:T(8,128)(2,1)S(1)} %copy-done.2, bf16[64,1024]{1,0:T(8,128)(2,1)S(1)} %copy-done.1), kind=kOutput, calls=%fused_computation.16 | convolution fusion | flops 201785344 | bytes 983040 | tf_op jit(solution)/shard_map/dot_general | solution.py:121
  (28 shorter events, 0.1 us)
Async XLA Ops:
  7.2 31.0 %copy-start = (bf16[256,4096]{1,0:T(8,128)(2,1)S(1)}, bf16[256,4096]{1,0:T(8,128)(2,1)}, u32[]{:S(2)}) copy-start(bf16[256,4096]{1,0:T(8,128)(2,1)} %param.36) | copy-start | bytes 6291460
  7.2 56.5 %reduce-scatter.3.cloned.1.call-start = ((), (), s32[]{:S(2)}) async-start(), calls=%async_computation.4 | async-start | bytes 655360 | tf_op jit(solution)/shard_map/reduce_scatter | solution.py:85
  25.7 3.5 %copy-start.8 = (f32[16,64]{1,0:T(8,128)S(1)}, f32[16,64]{1,0:T(8,128)}, u32[]{:S(2)}) copy-start(f32[16,64]{1,0:T(8,128)} %param.28) | copy-start | bytes 12292
  25.7 3.5 %copy-start.9 = (f32[16,64]{1,0:T(8,128)S(1)}, f32[16,64]{1,0:T(8,128)}, u32[]{:S(2)}) copy-start(f32[16,64]{1,0:T(8,128)} %param.27) | copy-start | bytes 12292
  25.7 3.7 %copy-start.3 = (f32[16,64,16]{1,2,0:T(8,128)S(1)}, f32[16,64,16]{1,2,0:T(8,128)}, u32[]{:S(2)}) copy-start(f32[16,64,16]{1,2,0:T(8,128)} %param.31) | copy-start | bytes 196612
  25.7 3.7 %copy-start.4 = (f32[16,64,16]{1,2,0:T(8,128)S(1)}, f32[16,64,16]{1,2,0:T(8,128)}, u32[]{:S(2)}) copy-start(f32[16,64,16]{1,2,0:T(8,128)} %param.30) | copy-start | bytes 196612
  29.2 1.5 copy-start.6
  29.4 2.3 %copy-start.5 = (f32[16,16,64]{2,1,0:T(8,128)S(1)}, f32[16,16,64]{2,1,0:T(8,128)}, u32[]{:S(2)}) copy-start(f32[16,16,64]{2,1,0:T(8,128)} %param.33) | copy-start | bytes 196612
  29.4 2.3 %copy-start.7 = (f32[16,16]{1,0:T(8,128)S(1)}, f32[16,16]{1,0:T(8,128)}, u32[]{:S(2)}) copy-start(f32[16,16]{1,0:T(8,128)} %param.34) | copy-start | bytes 3076
  32.7 8.2 %copy-start.10 = (s32[64,2]{0,1:T(2,128)S(1)}, s32[64,2]{0,1:T(2,128)}, u32[]{:S(2)}) copy-start(s32[64,2]{0,1:T(2,128)} %param.21) | copy-start | bytes 1540
  38.2 3.7 %copy-start.11 = (f32[64,2]{0,1:T(2,128)S(1)}, f32[64,2]{0,1:T(2,128)}, u32[]{:S(2)}) copy-start(f32[64,2]{0,1:T(2,128)} %param.22) | copy-start | bytes 1540
  38.2 25.5 %copy-start.1 = (bf16[64,1024]{1,0:T(8,128)(2,1)S(1)}, bf16[64,1024]{1,0:T(8,128)(2,1)}, u32[]{:S(2)}) copy-start(bf16[64,1024]{1,0:T(8,128)(2,1)} %param.20) | copy-start | bytes 393220
  38.2 32.3 %dynamic-slice-start = ((f32[4096]{0:T(1024)}, s32[]{:T(128)}), f32[1024]{0:T(1024)S(1)}, s32[]{:S(2)}) async-start(f32[4096]{0:T(1024)} %param.25, s32[]{:T(128)} %select_n.8), calls=%async_computation.7 | async-start | bytes 8704 | tf_op jit(solution)/shard_map/dynamic_slice | solution.py:90
  40.9 71.5 %all-gather.3.cloned.1.call-start = ((), (), s32[]{:S(2)}) async-start(), calls=%async_computation.6 | async-start | bytes 2621440 | tf_op jit(solution)/shard_map/all_gather | solution.py:104
  91.6 71.6 %reduce-scatter.5.cloned.1.call-start = ((), (), s32[]{:S(2)}) async-start(), calls=%async_computation.5 | async-start | bytes 2621440 | tf_op jit(solution)/shard_map/reduce_scatter | solution.py:116
  115.6 7.7 %slice-start = ((s8[11534336]{0:T(1024)(128)(4,1)}), s8[4194304]{0:T(1024)(128)(4,1)S(1)}, s32[]{:S(2)}) async-start(s8[11534336]{0:T(1024)(128)(4,1)} %bitcast.81), calls=%async_computation.8 | async-start | bytes 8388608
  116.5 6.8 %slice-start.1 = ((s8[11534336]{0:T(1024)(128)(4,1)}), s8[4194304]{0:T(1024)(128)(4,1)S(1)}, s32[]{:S(2)}) async-start(s8[11534336]{0:T(1024)(128)(4,1)} %bitcast.81), calls=%async_computation.9 | async-start | bytes 8388608
  116.5 7.0 %slice-start.2 = ((s8[11534336]{0:T(1024)(128)(4,1)}), s8[3145728]{0:T(1024)(128)(4,1)S(1)}, s32[]{:S(2)}) async-start(s8[11534336]{0:T(1024)(128)(4,1)} %bitcast.81), calls=%async_computation.10 | async-start | bytes 6291456
  116.6 10.5 %slice-start.3 = ((s8[11534336]{0:T(1024)(128)(4,1)}), s8[4194304]{0:T(1024)(128)(4,1)S(1)}, s32[]{:S(2)}) async-start(s8[11534336]{0:T(1024)(128)(4,1)} %bitcast.83), calls=%async_computation.11 | async-start | bytes 8388608
  116.6 10.5 %slice-start.4 = ((s8[11534336]{0:T(1024)(128)(4,1)}), s8[4194304]{0:T(1024)(128)(4,1)S(1)}, s32[]{:S(2)}) async-start(s8[11534336]{0:T(1024)(128)(4,1)} %bitcast.83), calls=%async_computation.12 | async-start | bytes 8388608
  123.6 3.5 %slice-start.5 = ((s8[11534336]{0:T(1024)(128)(4,1)}), s8[3145728]{0:T(1024)(128)(4,1)S(1)}, s32[]{:S(2)}) async-start(s8[11534336]{0:T(1024)(128)(4,1)} %bitcast.83), calls=%async_computation.13 | async-start | bytes 6291456
  163.1 19.9 %all-to-all-start.1 = ((bf16[8,32,1024]{2,1,0:T(8,128)(2,1)}), bf16[8,32,1024]{2,1,0:T(8,128)(2,1)}, u32[]{:S(2)}, u32[]{:S(2)}) async-start(bf16[8,32,1024]{2,1,0:T(8,128)(2,1)} %reduce-scatter.5.cloned.1.call-done), calls=%async_computation.3 | async-start | bytes 1048576 | tf_op jit(solution)/shard_map/all_to_all | solution.py:119
  168.6 14.4 %copy-start.2 = (bf16[64,1024]{1,0:T(8,128)(2,1)S(1)}, bf16[64,1024]{1,0:T(8,128)(2,1)}, u32[]{:S(2)}) copy-start(bf16[64,1024]{1,0:T(8,128)(2,1)} %reduce-scatter.3.cloned.1.call-done) | copy-start | bytes 393220
Sparse Core Ops, SparseCore 0:
  41.0 22.5 reduce-scatter.2
  91.7 20.6 all-gather.2
  131.9 31.1 reduce-scatter.4
